TPU v7x, 512 devices: a whole 4x8x8 slice. The times are simulated.
512 devices in a mesh: sp: 32 (over z, x), tp: 16 (over y, core).
Axes of the slice: x: 4, y: 8, z: 8, core: 2. Of those that a mesh axis runs over, the one named last changes fastest.
Arguments:
- outer_gate: bfloat16 [8192, 2048], P('sp', 'tp'), may hold values from -6 to 6
- inner_gate: bfloat16 [8192, 2048], P('sp', 'tp'), may hold values from -6 to 6
- conv_input: bfloat16 [8192, 2048], P('sp', 'tp'), may hold values from -6 to 6
- conv_weight: bfloat16 [3, 2048], P(None, 'tp'), may hold values from -3.5 to 3.5
- doc_ids: int32 [8192], P('sp'), may hold values from 0 to 15, as said below
- output_weight: bfloat16 [2048, 4096], P(None, 'tp'), may hold values from -0.125 to 0.125
- residual: bfloat16 [8192, 4096], P('sp', 'tp'), as said below
- norm_gain: bfloat16 [4096], P('tp'), may hold values from 0.099609375 to 1.8984375
- expert_ids: int32 [8192, 2], P('sp'), may hold values from 0 to 31, all different within a row; in each aligned block of 256 rows (0 to 255, 256 to 511, ...) at most 32 rows name the same one
- group_weight: float32 [8192], P('sp'), may hold values from 0.25 to 1
- expert_weight: float32 [8192, 2], P('sp'), may hold values from 0.05 to 1
- gate_weight: bfloat16 [32, 4096, 2048], P('sp', None, 'tp'), may hold values from -0.09375 to 0.09375
- up_weight: bfloat16 [32, 4096, 2048], P('sp', None, 'tp'), may hold values from -0.09375 to 0.09375
- down_weight: bfloat16 [32, 2048, 4096], P('sp', None, 'tp'), may hold values from -0.125 to 0.125
Outputs:
- layer_out: bfloat16 [8192, 4096], P('sp', 'tp')
Inputs may be any that keep to these rules, and one draw needn't show every extreme that they name: `expert_ids`: within the 256 rows of one index of sp no expert is named more than 32 times, a bound that some block reaches; the two experts of a row differ. `doc_ids`: never falling along positions, rising by one at each document's start; every document has 256 to 768 positions, and one exactly 768. `residual`: Columns' scales are of order one to ten.
All inputs are finite; a program needn't handle non-finite values.
Results may differ from a plain program's by a relative error of at most 0.009.
Values may be sent and summed in bfloat16 or wider, within the bound.
A program may use at most 64 MiB of HBM per device.

v0:
```python
import jax
import jax.numpy as jnp
from jax import lax
from jax.sharding import PartitionSpec as P

EPS = 1e-06


def passed_along(value, axis, steps):
    count = lax.axis_size(axis)
    initial, last = (max(0, -steps), min(count, count - steps))
    return lax.ppermute(value, axis, [(source, source + steps) for source in range(initial, last)])


def from_everyone(x, axis):
    copies = jnp.broadcast_to(x, (lax.axis_size(axis), *x.shape))
    return lax.all_to_all(copies, axis, split_axis=0, concat_axis=0, tiled=True)


def joined_along(blocks, dim):
    dims = list(blocks.shape[1:])
    dims[dim] *= blocks.shape[0]
    return jnp.moveaxis(blocks, 0, dim).reshape(dims)


def collect(x, axis, dim):
    blocks = from_everyone(x, axis)
    return joined_along(blocks, dim)


def of_everyone(x, axis):
    everything = from_everyone(x, axis)
    return jnp.sum(everything, axis=0)


def per_device(
    outer_gate,
    inner_gate,
    conv_input,
    conv_weight,
    doc_ids,
    output_weight,
    residual,
    norm_gain,
    expert_ids,
    group_weight,
    expert_weight,
    gate_weight,
    up_weight,
    down_weight,
):
    row_count = conv_input.shape[0]
    products = inner_gate.astype(jnp.float32) * conv_input.astype(jnp.float32)
    own_docs = doc_ids.astype(jnp.float32)
    tail_rows, tail_docs = passed_along((products[-2:], own_docs[-2:]), "sp", 1)
    ext_products = jnp.concatenate([tail_rows, products], axis=0)
    ext_docs = jnp.concatenate([tail_docs, own_docs], axis=0)
    taps = conv_weight.astype(jnp.float32)
    conv = taps[2] * products
    for shift_by in (1, 2):
        first = 2 - shift_by
        same_doc = (ext_docs[first : first + row_count] == own_docs)[:, None]
        conv = conv + jnp.where(
            same_doc, taps[2 - shift_by] * ext_products[first : first + row_count], 0.0
        )
    branch = (outer_gate.astype(jnp.float32) * conv).astype(jnp.bfloat16)
    cols_local = output_weight.shape[1]
    branch_sum = jnp.dot(
        collect(branch, "tp", 1), output_weight, preferred_element_type=jnp.float32
    )
    resid = (residual.astype(jnp.float32) + branch_sum).astype(jnp.bfloat16)
    resid_wide = resid.astype(jnp.float32)
    total_sq = of_everyone(jnp.sum(resid_wide * resid_wide, axis=1), "tp")
    width = cols_local * lax.axis_size("tp")
    scale = lax.rsqrt(total_sq / width + EPS)[:, None]
    normed = (resid_wide * scale * norm_gain.astype(jnp.float32)).astype(jnp.bfloat16)
    experts = lax.axis_size("sp")
    capacity = 4 * row_count // experts
    flat_experts = expert_ids.reshape(-1)
    onehot = (flat_experts[:, None] == jnp.arange(experts, dtype=jnp.int32)[None, :]).astype(
        jnp.int32
    )
    slot_rank = jnp.sum((jnp.cumsum(onehot, axis=0) - onehot) * onehot, axis=1)
    slot_index = flat_experts * capacity + slot_rank
    token_of = jnp.arange(2 * row_count, dtype=jnp.int32) // 2
    token_table = jnp.full((experts * capacity,), row_count, jnp.int32).at[slot_index].set(token_of)
    gate_local = gate_weight[0]
    up_local = up_weight[0]
    arrived_rows = experts * capacity
    padded = jnp.concatenate([normed, jnp.zeros((1, cols_local), jnp.bfloat16)], axis=0)
    outgoing = padded[token_table].reshape(experts, capacity, cols_local)
    arrived = lax.all_to_all(outgoing, "sp", split_axis=0, concat_axis=0, tiled=True).reshape(
        arrived_rows, cols_local
    )
    piece = lax.all_gather(arrived, "tp", axis=1, tiled=True)
    gate_val = jnp.dot(piece, gate_local, preferred_element_type=jnp.float32)
    up_val = jnp.dot(piece, up_local, preferred_element_type=jnp.float32)
    hidden = (jax.nn.silu(gate_val) * up_val).astype(jnp.bfloat16)
    down_local = down_weight[0]
    expert_out = jnp.dot(
        lax.all_gather(hidden, "tp", axis=1, tiled=True),
        down_local,
        preferred_element_type=jnp.float32,
    ).astype(jnp.bfloat16)
    returned = lax.all_to_all(
        expert_out.reshape(experts, capacity, cols_local),
        "sp",
        split_axis=0,
        concat_axis=0,
        tiled=True,
    )
    picked = (
        returned.reshape(arrived_rows, cols_local)[slot_index]
        .reshape(row_count, 2, cols_local)
        .astype(jnp.float32)
    )
    mix_weight = (
        group_weight[:, None] * expert_weight / jnp.sum(expert_weight, axis=1, keepdims=True)
    )
    routed_sum = jnp.sum(picked * mix_weight[:, :, None], axis=1)
    return (resid_wide + routed_sum).astype(jnp.bfloat16)


def solution(mesh):
    return jax.shard_map(
        per_device,
        mesh=mesh,
        in_specs=(
            P("sp", "tp"),
            P("sp", "tp"),
            P("sp", "tp"),
            P(None, "tp"),
            P("sp"),
            P(None, "tp"),
            P("sp", "tp"),
            P("tp"),
            P("sp", None),
            P("sp"),
            P("sp", None),
            P("sp", None, "tp"),
            P("sp", None, "tp"),
            P("sp", None, "tp"),
        ),
        out_specs=P("sp", "tp"),
        check_vma=False,
    )
```

profile of v0, /device:TPU:8, one launch (start us, length us, event | category | flops | bytes accessed | tf_op | source)
XLA Modules:
  0.0 263.7 jit_solution(17630297964401948509)
XLA Ops:
  6.5 0.8 convert_element_type.60
  7.4 3.4 %collective-permute-start = (f32[2]{0:T(128)S(1)}, f32[2]{0:T(128)S(1)}, u32[]{:S(2)}, u32[]{:S(2)}) collective-permute-start(f32[2]{0:T(128)S(1)} %slice.34), channel_id=1, source_target_pairs={{0,16},{16,32},{32,48},{48,64},{64,80},{80,96},{96,112},{112,128},... | collective-permute-start | bytes 32 | tf_op jit(solution)/shard_map/ppermute | solution.py:12
  10.8 0.9 convert_multiply_fusion
  11.7 3.4 %collective-permute-start.1 = (f32[2,128]{1,0:T(2,128)S(1)}, f32[2,128]{1,0:T(2,128)S(1)}, u32[]{:S(2)}, u32[]{:S(2)}) collective-permute-start(f32[2,128]{1,0:T(2,128)S(1)} %slice.48), channel_id=1, source_target_pairs={{0,16},{16,32},{32,48},{48,64},{64,80},{80,96},{96,112},{112,128},... | collective-permute-start | bytes 3080 | tf_op jit(solution)/shard_map/ppermute | solution.py:12
  15.1 0.7 convert_element_type.57
  15.9 0.8 slice_compare_fusion.1
  16.7 1.0 fusion.13
  17.8 1.1 broadcast_in_dim.44
  18.9 7.6 %all-to-all-start = ((bf16[16,256,128]{1,2,0:T(8,128)(2,1)}), bf16[16,256,128]{1,2,0:T(8,128)(2,1)S(1)}, u32[]{:S(2)}, u32[]{:S(2)}) async-start(bf16[16,256,128]{1,2,0:T(8,128)(2,1)} %broadcast_in_dim.44), calls=%async_computation | async-start | bytes 2097152 | tf_op jit(solution)/shard_map/all_to_all | solution.py:17
  26.4 0.8 copy.31
  27.5 1.2 reduce-window.6
  29.0 0.7 broadcast_multiply_fusion
  30.1 2.4 scatter_custom_fusion
  32.5 18.5 %all-to-all-done = bf16[16,256,128]{1,2,0:T(8,128)(2,1)S(1)} async-done(((bf16[16,256,128]{1,2,0:T(8,128)(2,1)}), bf16[16,256,128]{1,2,0:T(8,128)(2,1)S(1)}, u32[]{:S(2)}, u32[]{:S(2)}) %all-to-all-start) | async-done | bytes 1048608 | tf_op jit(solution)/shard_map/all_to_all | solution.py:17
  51.0 1.8 multiply_reduce_fusion.1
  52.8 0.6 broadcast_in_dim.45
  53.5 6.8 %all-to-all-start.1 = ((f32[16,1,256]{2,1,0:T(1,128)}), f32[16,1,256]{2,1,0:T(1,128)S(1)}, u32[]{:S(2)}, u32[]{:S(2)}) async-start(f32[16,1,256]{2,1,0:T(1,128)} %broadcast_in_dim.45), calls=%async_computation.1 | async-start | bytes 32768 | tf_op jit(solution)/shard_map/all_to_all | solution.py:17
  60.3 0.7 convert_element_type.64
  61.0 5.5 %all-to-all-done.1 = f32[16,1,256]{2,1,0:T(1,128)S(1)} async-done(((f32[16,1,256]{2,1,0:T(1,128)}), f32[16,1,256]{2,1,0:T(1,128)S(1)}, u32[]{:S(2)}, u32[]{:S(2)}) %all-to-all-start.1) | async-done | bytes 16416 | tf_op jit(solution)/shard_map/all_to_all | solution.py:17
  66.7 3.9 %gather_fusion = bf16[1024,256]{1,0:T(8,128)(2,1)S(1)} fusion(bf16[257,256]{1,0:T(8,128)(2,1)S(1)} %concatenate.11, s32[1024]{0:T(1024)S(1)} %fusion.20), kind=kCustom, calls=%fused_computation | custom fusion | bytes 1052672 | tf_op jit(solution)/shard_map/gather | solution.py:91
  70.7 32.5 %all_to_all.21 = bf16[32,32,256]{2,1,0:T(8,128)(2,1)} all-to-all(bf16[32,32,256]{2,1,0:T(8,128)(2,1)S(1)} %bitcast.51), channel_id=1, replica_groups=mesh['sp'=32,'tp'=16] {'sp'}, dimensions={0} | all-to-all | bytes 1048576 | tf_op jit(solution)/shard_map/all_to_all | solution.py:92
  103.2 58.8 %all-gather.3.cloned.1.call-done = bf16[1024,4096]{1,0:T(8,128)(2,1)} async-done(((bf16[1024,256]{1,0:T(8,128)(2,1)}), bf16[1024,4096]{1,0:T(8,128)(2,1)}) %all-gather.3.cloned.1.call-update) | async-done | bytes 8388624 | tf_op jit(solution)/shard_map/all_gather | solution.py:95
  162.0 5.9 %fusion.5 = f32[1024,128]{1,0:T(8,128)S(1)} fusion(bf16[1024,4096]{1,0:T(8,128)(2,1)} %all-gather.3.cloned.1.call-done, bf16[1,4096,128]{2,1,0:T(8,128)(2,1)S(1)} %copy-done.4), kind=kOutput, calls=%fused_computation.11 | convolution fusion | flops 1073741824 | bytes 9961472 | tf_op jit(solution)/shard_map/dot_general | solution.py:96
  168.0 3.0 %fusion = bf16[1024,128]{1,0:T(8,128)(2,1)} fusion(bf16[1024,4096]{1,0:T(8,128)(2,1)S(1)} %copy-done.3, bf16[1,4096,128]{2,1,0:T(8,128)(2,1)S(1)} %copy-done.5, f32[1024,128]{1,0:T(8,128)S(1)} %fusion.5), kind=kOutput, calls=%fused_computation.5 | convolution fusion | flops 1074528256 | bytes 10223616 | tf_op jit(solution)/shard_map/dot_general | solution.py:97
  171.0 49.6 %all-gather.5.cloned.1.call-done = bf16[1024,2048]{1,0:T(8,128)(2,1)} async-done(((bf16[1024,128]{1,0:T(8,128)(2,1)}), bf16[1024,2048]{1,0:T(8,128)(2,1)}) %all-gather.5.cloned.1.call-update) | async-done | bytes 4194320 | tf_op jit(solution)/shard_map/all_gather | solution.py:101
  220.6 4.2 %convolution_convert_fusion = bf16[1024,256]{1,0:T(8,128)(2,1)} fusion(bf16[1024,2048]{1,0:T(8,128)(2,1)} %all-gather.5.cloned.1.call-done, bf16[1,2048,256]{2,1,0:T(8,128)(2,1)S(1)} %copy-done), kind=kOutput, calls=%fused_computation.3 | convolution fusion | flops 1074003968 | bytes 5767168 | tf_op jit(solution)/shard_map/dot_general | solution.py:100
  224.9 10.2 %all-to-all-start.3 = ((bf16[32,32,256]{2,1,0:T(8,128)(2,1)}), bf16[32,32,256]{2,1,0:T(8,128)(2,1)S(1)}, u32[]{:S(2)}, u32[]{:S(2)}) async-start(bf16[32,32,256]{2,1,0:T(8,128)(2,1)} %bitcast.13), calls=%async_computation.3 | async-start | bytes 1048576 | tf_op jit(solution)/shard_map/all_to_all | solution.py:105
  235.3 18.0 %all-to-all-done.3 = bf16[32,32,256]{2,1,0:T(8,128)(2,1)S(1)} async-done(((bf16[32,32,256]{2,1,0:T(8,128)(2,1)}), bf16[32,32,256]{2,1,0:T(8,128)(2,1)S(1)}, u32[]{:S(2)}, u32[]{:S(2)}) %all-to-all-start.3) | async-done | bytes 524320 | tf_op jit(solution)/shard_map/all_to_all | solution.py:105
  253.3 1.9 gather_fusion.1
  255.2 0.3 reshape.85
  255.5 0.7 multiply_reduce_fusion
  256.2 0.7 add_convert_fusion
  (43 shorter events, 1.8 us)
Async XLA Ops:
  6.5 214.1 %copy-start = (bf16[1,2048,256]{2,1,0:T(8,128)(2,1)S(1)}, bf16[1,2048,256]{2,1,0:T(8,128)(2,1)}, u32[]{:S(2)}) copy-start(bf16[1,2048,256]{2,1,0:T(8,128)(2,1)} %param.27) | copy-start | bytes 3145732
  6.5 155.5 %copy-start.4 = (bf16[1,4096,128]{2,1,0:T(8,128)(2,1)S(1)}, bf16[1,4096,128]{2,1,0:T(8,128)(2,1)}, u32[]{:S(2)}) copy-start(bf16[1,4096,128]{2,1,0:T(8,128)(2,1)} %param.25) | copy-start | bytes 3145732
  7.4 8.4 %collective-permute-start = (f32[2]{0:T(128)S(1)}, f32[2]{0:T(128)S(1)}, u32[]{:S(2)}, u32[]{:S(2)}) collective-permute-start(f32[2]{0:T(128)S(1)} %slice.34), channel_id=1, source_target_pairs={{0,16},{16,32},{32,48},{48,64},{64,80},{80,96},{96,112},{112,128},... | collective-permute-start | bytes 32 | tf_op jit(solution)/shard_map/ppermute | solution.py:12
  11.7 4.9 %collective-permute-start.1 = (f32[2,128]{1,0:T(2,128)S(1)}, f32[2,128]{1,0:T(2,128)S(1)}, u32[]{:S(2)}, u32[]{:S(2)}) collective-permute-start(f32[2,128]{1,0:T(2,128)S(1)} %slice.48), channel_id=1, source_target_pairs={{0,16},{16,32},{32,48},{48,64},{64,80},{80,96},{96,112},{112,128},... | collective-permute-start | bytes 3080 | tf_op jit(solution)/shard_map/ppermute | solution.py:12
  18.9 32.2 %all-to-all-start = ((bf16[16,256,128]{1,2,0:T(8,128)(2,1)}), bf16[16,256,128]{1,2,0:T(8,128)(2,1)S(1)}, u32[]{:S(2)}, u32[]{:S(2)}) async-start(bf16[16,256,128]{1,2,0:T(8,128)(2,1)} %broadcast_in_dim.44), calls=%async_computation | async-start | bytes 2097152 | tf_op jit(solution)/shard_map/all_to_all | solution.py:17
  53.5 13.1 %all-to-all-start.1 = ((f32[16,1,256]{2,1,0:T(1,128)}), f32[16,1,256]{2,1,0:T(1,128)S(1)}, u32[]{:S(2)}, u32[]{:S(2)}) async-start(f32[16,1,256]{2,1,0:T(1,128)} %broadcast_in_dim.45), calls=%async_computation.1 | async-start | bytes 32768 | tf_op jit(solution)/shard_map/all_to_all | solution.py:17
  60.3 101.7 %all-gather.3.cloned.1.call-start = ((), (), s32[]{:S(2)}) async-start(), calls=%async_computation.4 | async-start | bytes 8912896 | tf_op jit(solution)/shard_map/all_gather | solution.py:95
  103.2 117.4 %all-gather.5.cloned.1.call-start = ((), (), s32[]{:S(2)}) async-start(), calls=%async_computation.5 | async-start | bytes 4456448 | tf_op jit(solution)/shard_map/all_gather | solution.py:101
  162.0 5.9 %copy-start.3 = (bf16[1024,4096]{1,0:T(8,128)(2,1)S(1)}, bf16[1024,4096]{1,0:T(8,128)(2,1)}, u32[]{:S(2)}) copy-start(bf16[1024,4096]{1,0:T(8,128)(2,1)} %all-gather.3.cloned.1.call-done) | copy-start | bytes 25165828
  162.0 6.0 %copy-start.5 = (bf16[1,4096,128]{2,1,0:T(8,128)(2,1)S(1)}, bf16[1,4096,128]{2,1,0:T(8,128)(2,1)}, u32[]{:S(2)}) copy-start(bf16[1,4096,128]{2,1,0:T(8,128)(2,1)} %param.26) | copy-start | bytes 3145732
  168.0 67.1 %copy-start.1 = (f32[256,2]{0,1:T(2,128)S(1)}, f32[256,2]{0,1:T(2,128)}, u32[]{:S(2)}) copy-start(f32[256,2]{0,1:T(2,128)} %param.24) | copy-start | bytes 6148
  168.0 67.1 %copy-start.2 = (f32[256]{0:T(256)S(1)}, f32[256]{0:T(256)}, u32[]{:S(2)}) copy-start(f32[256]{0:T(256)} %param.23) | copy-start | bytes 3076
  224.9 28.4 %all-to-all-start.3 = ((bf16[32,32,256]{2,1,0:T(8,128)(2,1)}), bf16[32,32,256]{2,1,0:T(8,128)(2,1)S(1)}, u32[]{:S(2)}, u32[]{:S(2)}) async-start(bf16[32,32,256]{2,1,0:T(8,128)(2,1)} %bitcast.13), calls=%async_computation.3 | async-start | bytes 1048576 | tf_op jit(solution)/shard_map/all_to_all | solution.py:105
Sparse Core Ops, SparseCore 0:
  103.3 58.6 all-gather.2
  171.2 49.4 all-gather.4
where the time goes:
time: 264 us
  waiting for transfers between devices  150 us (57%)
  blocking collectives  32.5 us (12%)
  starting transfers between devices  31.4 us (12%)
  matrix products  14.9 us (6%)
  between operations  13.6 us (5%)
  local copies, waits for them, and re-layouts  12.4 us (5%)
  other arithmetic  8.46 us (3%)
    all_gather x1, waiting for transfers between devices, per_device(): piece = lax.all_gather(arrived, 'tp', axis=1, tiled=True)  58.8 us
    all_gather x1, waiting for transfers between devices, per_device(): lax.all_gather(hidden, 'tp', axis=1, tiled=True)  49.6 us
    all_to_all x1, blocking collectives, per_device(): lax.all_to_all(outgoing, 'sp', split_axis=0, concat_axis=0, tiled=True)  32.5 us
    all_to_all x2, waiting for transfers between devices, from_everyone(): return lax.all_to_all(copies, axis, split_axis=0, concat_axis=0, tiled=True)  24 us
    all_to_all x1, waiting for transfers between devices, per_device(): lax.all_to_all(expert_out.reshape(experts, capacity, cols_local), 'sp', s...  18 us
    all_to_all x2, starting transfers between devices, from_everyone(): return lax.all_to_all(copies, axis, split_axis=0, concat_axis=0, tiled=True)  14.4 us
    all_to_all x1, starting transfers between devices, per_device(): lax.all_to_all(expert_out.reshape(experts, capacity, cols_local), 'sp', s...  10.2 us
    ppermute x2, starting transfers between devices, passed_along(): lax.ppermute(value, axis, [(source, source + steps) for source in range(i...  6.78 us
  transfers between devices with their start and end apart: 7, of which 5 were waited for; matrix products, arithmetic and copies ran while one was open for 4% of the time, Pallas kernels for 0%

commit v1 on v0

--- a/solution.py
+++ b/solution.py
@@ -4,6 +4,11 @@
 from jax.sharding import PartitionSpec as P
 
 EPS = 1e-06
+
+
+def gather_from_all(x, axis, dim):
+    copies = jnp.concatenate([x] * lax.axis_size(axis), axis=dim)
+    return lax.all_to_all(copies, axis, dim, dim, tiled=True)
 
 
 def passed_along(value, axis, steps):
@@ -98,9 +103,7 @@
     hidden = (jax.nn.silu(gate_val) * up_val).astype(jnp.bfloat16)
     down_local = down_weight[0]
     expert_out = jnp.dot(
-        lax.all_gather(hidden, "tp", axis=1, tiled=True),
-        down_local,
-        preferred_element_type=jnp.float32,
+        gather_from_all(hidden, "tp", 1), down_local, preferred_element_type=jnp.float32
     ).astype(jnp.bfloat16)
     returned = lax.all_to_all(
         expert_out.reshape(experts, capacity, cols_local),

time: 264 us -> 313 us (1.19)
  the two profiles are of different devices: /device:TPU:8 before, /device:TPU:1 now
where the time goes in v1:
time: 313 us
  blocking collectives  131 us (42%)
  waiting for transfers between devices  109 us (35%)
  starting transfers between devices  26 us (8%)
  between operations  13.8 us (4%)
  matrix products  13.3 us (4%)
  local copies, waits for them, and re-layouts  12.6 us (4%)
  other arithmetic  7.06 us (2%)
    all_to_all x1, blocking collectives, gather_from_all(): return lax.all_to_all(copies, axis, dim, dim, tiled=True)  100 us
    all_gather x1, waiting for transfers between devices, per_device(): piece = lax.all_gather(arrived, 'tp', axis=1, tiled=True)  62.4 us
    all_to_all x1, blocking collectives, per_device(): lax.all_to_all(outgoing, 'sp', split_axis=0, concat_axis=0, tiled=True)  30.8 us
    all_to_all x2, waiting for transfers between devices, from_everyone(): return lax.all_to_all(copies, axis, split_axis=0, concat_axis=0, tiled=True)  29.8 us
    all_to_all x1, waiting for transfers between devices, per_device(): lax.all_to_all(expert_out.reshape(experts, capacity, cols_local), 'sp', s...  16.8 us
    all_to_all x2, starting transfers between devices, from_everyone(): return lax.all_to_all(copies, axis, split_axis=0, concat_axis=0, tiled=True)  11.8 us
    all_to_all x1, starting transfers between devices, per_device(): lax.all_to_all(expert_out.reshape(experts, capacity, cols_local), 'sp', s...  7.14 us
    ppermute x2, starting transfers between devices, passed_along(): lax.ppermute(value, axis, [(source, source + steps) for source in range(i...  7.04 us
  transfers between devices with their start and end apart: 6, of which 4 were waited for; matrix products, arithmetic and copies ran while one was open for 3% of the time, Pallas kernels for 0%

profile of v1, /device:TPU:1, one launch (start us, length us, event | category | flops | bytes accessed | tf_op | source)
XLA Modules:
  0.0 312.5 jit_solution(3647369513853047622)
XLA Ops:
  6.5 0.8 convert_element_type.60
  7.4 3.9 %collective-permute-start = (f32[2]{0:T(128)S(1)}, f32[2]{0:T(128)S(1)}, u32[]{:S(2)}, u32[]{:S(2)}) collective-permute-start(f32[2]{0:T(128)S(1)} %slice.34), channel_id=1, source_target_pairs={{0,16},{16,32},{32,48},{48,64},{64,80},{80,96},{96,112},{112,128},... | collective-permute-start | bytes 32 | tf_op jit(solution)/shard_map/ppermute | solution.py:17
  11.3 0.9 convert_multiply_fusion
  12.2 3.1 collective-permute-start.1
  15.4 0.7 convert_element_type.57
  16.1 0.8 slice_compare_fusion.1
  16.9 1.0 fusion.13
  18.0 1.1 broadcast_in_dim.44
  19.1 8.3 %all-to-all-start = ((bf16[16,256,128]{1,2,0:T(8,128)(2,1)}), bf16[16,256,128]{1,2,0:T(8,128)(2,1)S(1)}, u32[]{:S(2)}, u32[]{:S(2)}) async-start(bf16[16,256,128]{1,2,0:T(8,128)(2,1)} %broadcast_in_dim.44), calls=%async_computation | async-start | bytes 2097152 | tf_op jit(solution)/shard_map/all_to_all | solution.py:22
  27.4 0.8 copy.31
  28.5 1.2 reduce-window.6
  29.7 0.2 slice_reduce_fusion
  30.1 0.1 mul.115
  30.4 2.4 scatter_custom_fusion
  32.9 22.6 %all-to-all-done = bf16[16,256,128]{1,2,0:T(8,128)(2,1)S(1)} async-done(((bf16[16,256,128]{1,2,0:T(8,128)(2,1)}), bf16[16,256,128]{1,2,0:T(8,128)(2,1)S(1)}, u32[]{:S(2)}, u32[]{:S(2)}) %all-to-all-start) | async-done | bytes 1048608 | tf_op jit(solution)/shard_map/all_to_all | solution.py:22
  55.4 1.9 multiply_reduce_fusion.1
  57.3 0.6 broadcast_in_dim.45
  57.9 3.4 %all-to-all-start.1 = ((f32[16,1,256]{2,1,0:T(1,128)}), f32[16,1,256]{2,1,0:T(1,128)S(1)}, u32[]{:S(2)}, u32[]{:S(2)}) async-start(f32[16,1,256]{2,1,0:T(1,128)} %broadcast_in_dim.45), calls=%async_computation.1 | async-start | bytes 32768 | tf_op jit(solution)/shard_map/all_to_all | solution.py:22
  61.4 7.3 %all-to-all-done.1 = f32[16,1,256]{2,1,0:T(1,128)S(1)} async-done(((f32[16,1,256]{2,1,0:T(1,128)}), f32[16,1,256]{2,1,0:T(1,128)S(1)}, u32[]{:S(2)}, u32[]{:S(2)}) %all-to-all-start.1) | async-done | bytes 16416 | tf_op jit(solution)/shard_map/all_to_all | solution.py:22
  68.9 3.9 %gather_fusion = bf16[1024,256]{1,0:T(8,128)(2,1)S(1)} fusion(bf16[257,256]{1,0:T(8,128)(2,1)S(1)} %concatenate.14, s32[1024]{0:T(1024)S(1)} %fusion.20), kind=kCustom, calls=%fused_computation | custom fusion | bytes 1052672 | tf_op jit(solution)/shard_map/gather | solution.py:96
  72.8 30.8 %all_to_all.33 = bf16[32,32,256]{2,1,0:T(8,128)(2,1)} all-to-all(bf16[32,32,256]{2,1,0:T(8,128)(2,1)S(1)} %bitcast.57), channel_id=1, replica_groups=mesh['sp'=32,'tp'=16] {'sp'}, dimensions={0} | all-to-all | bytes 1048576 | tf_op jit(solution)/shard_map/all_to_all | solution.py:97
  103.6 62.4 %all-gather.2.cloned.1.call-done = bf16[1024,4096]{1,0:T(8,128)(2,1)} async-done(((bf16[1024,256]{1,0:T(8,128)(2,1)}), bf16[1024,4096]{1,0:T(8,128)(2,1)}) %all-gather.2.cloned.1.call-update) | async-done | bytes 8388624 | tf_op jit(solution)/shard_map/all_gather | solution.py:100
  166.0 6.4 %fusion.5 = f32[1024,128]{0,1:T(8,128)S(1)} fusion(bf16[1024,4096]{1,0:T(8,128)(2,1)} %all-gather.2.cloned.1.call-done, bf16[1,4096,128]{2,1,0:T(8,128)(2,1)S(1)} %copy-done.2), kind=kOutput, calls=%fused_computation.11 | convolution fusion | flops 1073741824 | bytes 9961472 | tf_op jit(solution)/shard_map/dot_general | solution.py:101
  172.5 2.9 constant_dynamic-update-slice_fusion.15
  175.8 100.0 %all_to_all.34 = bf16[1024,16,128]{0,2,1:T(8,128)(2,1)S(1)} all-to-all(bf16[1024,16,128]{0,2,1:T(8,128)(2,1)S(1)} %bitcast.53), channel_id=1, replica_groups=mesh['sp'=32,'tp'=16] {'tp'}, dimensions={1} | all-to-all | bytes 8388608 | tf_op jit(solution)/shard_map/all_to_all | solution.py:11
  275.8 2.1 convolution_convert_fusion
  277.9 7.1 %all-to-all-start.4 = ((bf16[32,32,256]{2,1,0:T(8,128)(2,1)}), bf16[32,32,256]{2,1,0:T(8,128)(2,1)S(1)}, u32[]{:S(2)}, u32[]{:S(2)}) async-start(bf16[32,32,256]{2,1,0:T(8,128)(2,1)} %bitcast.15), calls=%async_computation.4 | async-start | bytes 1048576 | tf_op jit(solution)/shard_map/all_to_all | solution.py:108
  285.3 16.8 %all-to-all-done.4 = bf16[32,32,256]{2,1,0:T(8,128)(2,1)S(1)} async-done(((bf16[32,32,256]{2,1,0:T(8,128)(2,1)}), bf16[32,32,256]{2,1,0:T(8,128)(2,1)S(1)}, u32[]{:S(2)}, u32[]{:S(2)}) %all-to-all-start.4) | async-done | bytes 524320 | tf_op jit(solution)/shard_map/all_to_all | solution.py:108
  302.1 1.9 gather_fusion.1
  304.0 0.3 reshape.87
  304.3 0.7 multiply_reduce_fusion
  305.0 0.7 add_convert_fusion
  (62 shorter events, 1.6 us)
Async XLA Ops:
  6.5 165.9 %copy-start = (bf16[1,4096,128]{2,1,0:T(8,128)(2,1)S(1)}, bf16[1,4096,128]{2,1,0:T(8,128)(2,1)}, u32[]{:S(2)}) copy-start(bf16[1,4096,128]{2,1,0:T(8,128)(2,1)} %param.26) | copy-start | bytes 3145732
  6.5 23.4 %copy-start.4 = (s32[256,2]{0,1:T(2,128)S(1)}, s32[256,2]{0,1:T(2,128)}, u32[]{:S(2)}) copy-start(s32[256,2]{0,1:T(2,128)} %param.22) | copy-start | bytes 6148
  6.5 48.9 %copy-start.3 = (bf16[256,256]{1,0:T(8,128)(2,1)S(1)}, bf16[256,256]{1,0:T(8,128)(2,1)}, u32[]{:S(2)}) copy-start(bf16[256,256]{1,0:T(8,128)(2,1)} %param.20) | copy-start | bytes 393220
  6.5 54.9 %copy-start.8 = (bf16[256]{0:T(256)(128)(2,1)S(1)}, bf16[256]{0:T(256)(128)(2,1)}, u32[]{:S(2)}) copy-start(bf16[256]{0:T(256)(128)(2,1)} %param.21) | copy-start | bytes 1540
  7.4 8.7 %collective-permute-start = (f32[2]{0:T(128)S(1)}, f32[2]{0:T(128)S(1)}, u32[]{:S(2)}, u32[]{:S(2)}) collective-permute-start(f32[2]{0:T(128)S(1)} %slice.34), channel_id=1, source_target_pairs={{0,16},{16,32},{32,48},{48,64},{64,80},{80,96},{96,112},{112,128},... | collective-permute-start | bytes 32 | tf_op jit(solution)/shard_map/ppermute | solution.py:17
  12.2 4.7 %collective-permute-start.1 = (f32[2,128]{1,0:T(2,128)S(1)}, f32[2,128]{1,0:T(2,128)S(1)}, u32[]{:S(2)}, u32[]{:S(2)}) collective-permute-start(f32[2,128]{1,0:T(2,128)S(1)} %slice.48), channel_id=1, source_target_pairs={{0,16},{16,32},{32,48},{48,64},{64,80},{80,96},{96,112},{112,128},... | collective-permute-start | bytes 3080 | tf_op jit(solution)/shard_map/ppermute | solution.py:17
  19.1 36.3 %all-to-all-start = ((bf16[16,256,128]{1,2,0:T(8,128)(2,1)}), bf16[16,256,128]{1,2,0:T(8,128)(2,1)S(1)}, u32[]{:S(2)}, u32[]{:S(2)}) async-start(bf16[16,256,128]{1,2,0:T(8,128)(2,1)} %broadcast_in_dim.44), calls=%async_computation | async-start | bytes 2097152 | tf_op jit(solution)/shard_map/all_to_all | solution.py:22
  55.4 110.6 %copy-start.2 = (bf16[1,4096,128]{2,1,0:T(8,128)(2,1)S(1)}, bf16[1,4096,128]{2,1,0:T(8,128)(2,1)}, u32[]{:S(2)}) copy-start(bf16[1,4096,128]{2,1,0:T(8,128)(2,1)} %param.25) | copy-start | bytes 3145732
  57.9 10.8 %all-to-all-start.1 = ((f32[16,1,256]{2,1,0:T(1,128)}), f32[16,1,256]{2,1,0:T(1,128)S(1)}, u32[]{:S(2)}, u32[]{:S(2)}) async-start(f32[16,1,256]{2,1,0:T(1,128)} %broadcast_in_dim.45), calls=%async_computation.1 | async-start | bytes 32768 | tf_op jit(solution)/shard_map/all_to_all | solution.py:22
  61.3 104.7 %all-gather.2.cloned.1.call-start = ((), (), s32[]{:S(2)}) async-start(), calls=%async_computation.5 | async-start | bytes 8912896 | tf_op jit(solution)/shard_map/all_gather | solution.py:100
  166.0 6.4 %copy-start.1 = (bf16[1024,4096]{1,0:T(8,128)(2,1)S(1)}, bf16[1024,4096]{1,0:T(8,128)(2,1)}, u32[]{:S(2)}) copy-start(bf16[1024,4096]{1,0:T(8,128)(2,1)} %all-gather.2.cloned.1.call-done) | copy-start | bytes 25165828
  175.8 100.0 %copy-start.7 = (bf16[1,2048,256]{2,1,0:T(8,128)(2,1)S(1)}, bf16[1,2048,256]{2,1,0:T(8,128)(2,1)}, u32[]{:S(2)}) copy-start(bf16[1,2048,256]{2,1,0:T(8,128)(2,1)} %param.27) | copy-start | bytes 3145732
  275.8 9.3 %copy-start.5 = (f32[256,2]{0,1:T(2,128)S(1)}, f32[256,2]{0,1:T(2,128)}, u32[]{:S(2)}) copy-start(f32[256,2]{0,1:T(2,128)} %param.24) | copy-start | bytes 6148
  275.8 9.3 %copy-start.6 = (f32[256]{0:T(256)S(1)}, f32[256]{0:T(256)}, u32[]{:S(2)}) copy-start(f32[256]{0:T(256)} %param.23) | copy-start | bytes 3076
  277.9 24.1 %all-to-all-start.4 = ((bf16[32,32,256]{2,1,0:T(8,128)(2,1)}), bf16[32,32,256]{2,1,0:T(8,128)(2,1)S(1)}, u32[]{:S(2)}, u32[]{:S(2)}) async-start(bf16[32,32,256]{2,1,0:T(8,128)(2,1)} %bitcast.15), calls=%async_computation.4 | async-start | bytes 1048576 | tf_op jit(solution)/shard_map/all_to_all | solution.py:108
Sparse Core Ops, SparseCore 0:
  103.7 62.2 all-gather.1
